TPU v7x, 32 devices: a whole 2x2x4 slice. The times are simulated.
32 devices in a mesh: fs: 8 (over z, y), tp: 4 (over x, core).
Axes of the slice: x: 2, y: 2, z: 4, core: 2. Of those that a mesh axis runs over, the one named last changes fastest.
Arguments:
- tokens: bfloat16 [3072, 2048], P('tp'), may hold values from -6 to 6
- norm_gain: float32 [2048], P('fs'), may hold values from 0.1 to 1.9
- gate_weight: float32 [4, 2048, 8192], P(None, 'fs', 'tp'), may hold values from -0.125 to 0.125
- up_weight: float32 [4, 2048, 8192], P(None, 'fs', 'tp'), may hold values from -0.125 to 0.125
- down_weight: float32 [4, 8192, 2048], P(None, 'fs', 'tp'), may hold values from -0.0625 to 0.0625
- routes: int32 [3072, 2], P('tp'), may hold values from 0 to 3, all different within a row; in each aligned block of 768 rows (0 to 767, 768 to 1535, ...) at most 480 rows name the same one
- route_logit: float32 [3072, 2], P('tp'), may hold values from -6 to 6
Outputs:
- gate_out: bfloat16 [4, 2048, 8192], P(None, None, 'fs')
- up_out: bfloat16 [4, 2048, 8192], P(None, None, 'fs')
- down_out: bfloat16 [4, 8192, 2048], P(None, 'fs')
- mixed: bfloat16 [3072, 2048], P(('tp', 'fs'))
Inputs may be any that keep to these rules, and one draw needn't show every extreme that they name: `routes`: the two experts of a token differ. In each aligned block of 768 tokens (the tokens of one request group) every expert is named by at most 480 tokens, a bound that some block reaches.
All inputs are finite; a program needn't handle non-finite values.
Results may differ from a plain program's by a relative error of at most 0.0082.
Values may be sent and summed in bfloat16 or wider, within the bound.
No kernel may reach another device: no remote copies, remote signals or barrier semaphores. Data moves between devices by JAX's collectives and lax.ppermute only.
A program may use at most 192 MiB of HBM per device.

v0:
```python
import jax
import jax.numpy as jnp
from jax import lax
from jax.sharding import PartitionSpec as P

EPS = 0.5


def shards(tokens, norm_gain, gate_weight, up_weight, down_weight, routes, route_logit):
    gain_col = norm_gain[None, :, None]
    gate_part = (gate_weight * gain_col).astype(jnp.bfloat16)
    up_part = (up_weight * gain_col).astype(jnp.bfloat16)
    down_part = down_weight.astype(jnp.bfloat16)
    gate_one, up_one = (
        lax.all_to_all(gate_part, "tp", split_axis=0, concat_axis=2, tiled=True),
        lax.all_to_all(up_part, "tp", split_axis=0, concat_axis=2, tiled=True),
    )
    gate_mine, up_mine = (
        lax.all_to_all(gate_one, "fs", split_axis=2, concat_axis=1, tiled=True),
        lax.all_to_all(up_one, "fs", split_axis=2, concat_axis=1, tiled=True),
    )
    gate_out, up_out = (
        lax.all_gather(gate_mine, "tp", axis=0, tiled=True),
        lax.all_gather(up_mine, "tp", axis=0, tiled=True),
    )
    down_out = lax.all_gather(down_part, "tp", axis=2, tiled=True)
    total_rows = tokens.shape[0]
    width = tokens.shape[1]
    experts = gate_out.shape[0]
    capacity = total_rows * 5 // 8
    floats = tokens.astype(jnp.float32)
    normed = (floats * lax.rsqrt(jnp.mean(floats * floats, axis=1, keepdims=True) + EPS)).astype(
        jnp.bfloat16
    )
    first_share = jax.nn.sigmoid(route_logit[:, 0] - route_logit[:, 1])
    shares = jnp.stack([first_share, 1.0 - first_share], axis=1)
    chosen = (routes[:, :, None] == jnp.arange(experts, dtype=jnp.int32)[None, None, :]).astype(
        jnp.int32
    )
    counts = jnp.sum(chosen, axis=1)
    before = jnp.cumsum(counts, axis=0) - counts
    slot_index = jnp.sum(chosen * before[:, None, :], axis=2)
    flat_slot = routes * capacity + slot_index
    row_ids = jnp.repeat(jnp.arange(total_rows, dtype=jnp.int32), 2)
    table = (
        jnp.full((experts * capacity,), total_rows, jnp.int32)
        .at[flat_slot.reshape(-1)]
        .set(row_ids)
    )
    gathered = jnp.take(normed, table, axis=0, mode="fill", fill_value=0).reshape(
        experts, capacity, width
    )
    gate_val = jnp.einsum("ecd,edf->ecf", gathered, gate_out, preferred_element_type=jnp.float32)
    up_val = jnp.einsum("ecd,edf->ecf", gathered, up_out, preferred_element_type=jnp.float32)
    hidden = (jax.nn.silu(gate_val) * up_val).astype(jnp.bfloat16)
    results = jnp.einsum("ecf,efd->ecd", hidden, down_out, preferred_element_type=jnp.float32)
    flat_rows = results.reshape(experts * capacity, width)
    first_rows = jnp.take(flat_rows, flat_slot[:, 0], axis=0)
    second_rows = jnp.take(flat_rows, flat_slot[:, 1], axis=0)
    mixed = lax.psum_scatter(
        shares[:, 0:1] * first_rows + shares[:, 1:2] * second_rows,
        "fs",
        scatter_dimension=0,
        tiled=True,
    )
    return (gate_out, up_out, down_out, mixed.astype(jnp.bfloat16))


def solution(mesh):
    return jax.shard_map(
        shards,
        mesh=mesh,
        in_specs=(
            P("tp", None),
            P("fs"),
            P(None, "fs", "tp"),
            P(None, "fs", "tp"),
            P(None, "fs", "tp"),
            P("tp", None),
            P("tp", None),
        ),
        out_specs=(
            P(None, None, "fs"),
            P(None, None, "fs"),
            P(None, "fs", None),
            P(("tp", "fs"), None),
        ),
        check_vma=False,
    )
```

profile of v0, /device:TPU:0, one launch (start us, length us, event | category | flops | bytes accessed | tf_op | source)
XLA Modules:
  0.0 959.0 jit_solution(9687158230475078291)
XLA Ops:
  7.2 0.0 all-gather.6.cloned.1.call-start
  7.2 8.7 copy.43
  15.9 0.0 copy-start.3
  15.9 8.7 copy.46
  24.6 0.0 copy-done.3
  24.6 10.7 %multiply_convert_fusion = (bf16[4,256,2048]{1,2,0:T(8,128)(2,1)}, bf16[4,256,2048]{1,2,0:T(8,128)(2,1)}) fusion(f32[4,256,2048]{1,2,0:T(8,128)} %copy.46, f32[256]{0:T(256)S(1)} %copy-done.3, f32[4,256,2048]{1,2,0:T(8,128)} %copy.43), kind=kLoop, calls=%fused_computation.4 | loop fusion | flops 8388608 | bytes 25166848 | tf_op jit(solution)/shard_map/convert_element_type | solution.py:12
  35.3 52.6 %all_to_all.72 = bf16[4,256,2048]{1,2,0:T(8,128)(2,1)S(1)} all-to-all(bf16[4,256,2048]{1,2,0:T(8,128)(2,1)} %get-tuple-element.9), channel_id=1, replica_groups=mesh['fs'=8,'tp'=4] {'tp'}, dimensions={0} | all-to-all | bytes 8388608 | tf_op jit(solution)/shard_map/all_to_all | solution.py:16
  87.9 49.3 %copy.56 = bf16[1,256,8192]{1,0,2:T(2,128)(2,1)} copy(bf16[1,256,8192]{1,2,0:T(8,128)(2,1)S(1)} %bitcast.49) | data formatting | bytes 8388608 | tf_op jit(solution)/shard_map/all_to_all | solution.py:16
  137.2 0.5 broadcast.78
  137.7 43.5 %reduce.13 = bf16[8192,256]{1,0:T(8,128)(2,1)} reduce(bf16[8192,1,256]{2,1,0:T(2,128)(2,1)} %bitcast.45, bf16[]{:T(256)} %broadcast.78), dimensions={1}, to_apply=%bitcast.40.reduce_sub_computation | reduce | bytes 8388610
  181.2 6.9 reshape.137
  188.2 99.8 %all_to_all.73 = bf16[8,2,131072]{2,1,0:T(2,128)(2,1)} all-to-all(bf16[8,2,131072]{2,1,0:T(2,128)(2,1)} %reshape.137), channel_id=1, replica_groups=mesh['fs'=8,'tp'=4] {'fs'}, dimensions={0} | all-to-all | bytes 8388608 | tf_op jit(solution)/shard_map/all_to_all | solution.py:20
  288.0 8.7 reshape.138
  296.7 6.1 copy.51
  302.8 6.4 copy.48
  309.3 0.0 all-gather.6.cloned.1.call-update
  309.3 0.0 all-gather.8.cloned.1.call-start
  309.3 6.0 convert_element_type.26
  315.4 0.0 all-gather.8.cloned.1.call-update
  315.4 0.0 all-gather.4.cloned.1.call-start
  315.4 97.4 %all_to_all.74 = bf16[4,256,2048]{1,2,0:T(8,128)(2,1)S(1)} all-to-all(bf16[4,256,2048]{1,2,0:T(8,128)(2,1)} %get-tuple-element.10), channel_id=1, replica_groups=mesh['fs'=8,'tp'=4] {'tp'}, dimensions={0} | all-to-all | bytes 8388608 | tf_op jit(solution)/shard_map/all_to_all | solution.py:15
  412.8 49.3 %copy.57 = bf16[1,256,8192]{1,0,2:T(2,128)(2,1)} copy(bf16[1,256,8192]{1,2,0:T(8,128)(2,1)S(1)} %bitcast.51) | data formatting | bytes 8388608 | tf_op jit(solution)/shard_map/all_to_all | solution.py:15
  462.2 43.5 %reduce.12 = bf16[8192,256]{1,0:T(8,128)(2,1)} reduce(bf16[8192,1,256]{2,1,0:T(2,128)(2,1)} %bitcast.46, bf16[]{:T(256)} %broadcast.78), dimensions={1}, to_apply=%bitcast.41.reduce_sub_computation | reduce | bytes 8388610
  505.7 7.0 reshape.135
  512.7 97.7 %all_to_all.75 = bf16[8,2,131072]{2,1,0:T(2,128)(2,1)} all-to-all(bf16[8,2,131072]{2,1,0:T(2,128)(2,1)} %reshape.135), channel_id=1, replica_groups=mesh['fs'=8,'tp'=4] {'fs'}, dimensions={0} | all-to-all | bytes 8388608 | tf_op jit(solution)/shard_map/all_to_all | solution.py:19
  610.4 8.7 reshape.136
  619.1 6.1 copy.50
  625.2 0.0 copy-start.1
  625.2 6.6 copy.45
  631.8 0.0 all-gather.4.cloned.1.call-update
  631.8 0.0 reduce-scatter.2.cloned.1.call-start
  631.9 0.0 copy-done.1
  631.9 1.1 reduce-window.6
  633.1 0.2 slice_reduce_fusion
  633.3 0.2 reduce-window.9
  633.5 0.1 add_bitcast_fusion
  633.6 0.2 copy.49
  633.8 0.3 reshape.85
  634.1 0.8 reshape.116
  634.9 6.3 scatter_custom_fusion
  641.3 0.1 broadcast_in_dim.37
  641.4 0.0 copy-done
  641.4 0.7 fusion.2
  642.1 2.8 fusion.3
  644.9 0.0 copy-start.2
  644.9 8.9 gather_fusion
  653.9 0.0 copy-done.2
  653.9 0.0 all-gather.6.cloned.1.call-done
  654.0 16.3 %fusion = f32[4,480,1024]{2,1,0:T(8,128)} fusion(bf16[4,2048,1024]{2,1,0:T(8,128)(2,1)} %all-gather.6.cloned.1.call-done, bf16[4,480,2048]{2,1,0:T(8,128)(2,1)} %bitcast.57, pred[4,480]{1,0:T(4,128)(4,1)S(1)} %broadcast_in_dim.37), kind=kOutput, calls=%fused_computation.10 | convolution fusion | flops 8056995840 | bytes 32507776 | tf_op jit(solution)/shard_map/ecd,edf->ecf/dot_general | solution.py:54
  670.2 65.7 %all-gather.4.cloned.1.call-done = bf16[4,2048,1024]{2,1,0:T(8,128)(2,1)} async-done(((bf16[1,2048,1024]{2,1,0:T(8,128)(2,1)}), bf16[4,2048,1024]{2,1,0:T(8,128)(2,1)}) %all-gather.4.cloned.1.call-update) | async-done | bytes 16777232 | tf_op jit(solution)/shard_map/all_gather | solution.py:23
  735.9 27.2 %fusion.7 = f32[4,480,2048]{2,1,0:T(8,128)} fusion(bf16[4,1024,2048]{2,1,0:T(8,128)(2,1)} %all-gather.8.cloned.1.call-done, f32[4,480,1024]{2,1,0:T(8,128)} %fusion, bf16[4,2048,1024]{2,1,0:T(8,128)(2,1)} %all-gather.4.cloned.1.call-done, bf16[4,480,2048]{2,1,0:T(8,128)(2,1)} %bitcast.58, pred[4,480]{1,0:T(4,128)(4,1)S(1)} %broadcast_in_dim.37), kind=kOutput, calls=%fused_computation.19 | convolution fusion | flops 16121856000 | bytes 65013632 | tf_op jit(solution)/shard_map/ecf,efd->ecd/dot_general | solution.py:56
  763.1 12.7 %gather_fusion.1 = f32[768,2048]{1,0:T(8,128)} fusion(f32[1920,2048]{1,0:T(8,128)} %bitcast.43, s32[1024]{0:T(1024)S(1)} %pad_clamp_fusion.2), kind=kCustom, calls=%fused_computation.clone | custom fusion | bytes 12585984 | tf_op jit(solution)/shard_map/jit(_take)/gather | solution.py:58
  775.8 12.7 %gather_fusion.2 = f32[768,2048]{1,0:T(8,128)} fusion(f32[1920,2048]{1,0:T(8,128)} %bitcast.44, s32[1024]{0:T(1024)S(1)} %pad_clamp_fusion.1), kind=kCustom, calls=%fused_computation.1.clone | custom fusion | bytes 12585984 | tf_op jit(solution)/shard_map/jit(_take)/gather | solution.py:59
  788.5 7.2 fusion.4
  795.7 0.0 reduce-scatter.2.cloned.1.call-update
  795.7 118.2 %reduce-scatter.2.cloned.1.call-done = f32[96,2048]{1,0:T(8,128)} async-done(((f32[768,2048]{1,0:T(8,128)}), f32[96,2048]{1,0:T(8,128)}) %reduce-scatter.2.cloned.1.call-update) | async-done | bytes 786448 | tf_op jit(solution)/shard_map/reduce_scatter | solution.py:60
  913.9 1.9 convert_element_type.31
  915.8 15.2 %copy.61 = bf16[4,2048,1024]{2,1,0:T(8,128)(2,1)} copy(bf16[4,2048,1024]{2,1,0:T(8,128)(2,1)} %all-gather.4.cloned.1.call-done) | data formatting | bytes 33554432
  931.1 15.2 %copy.62 = bf16[4,2048,1024]{2,1,0:T(8,128)(2,1)} copy(bf16[4,2048,1024]{2,1,0:T(8,128)(2,1)} %all-gather.6.cloned.1.call-done) | data formatting | bytes 33554432
  946.3 0.0 slice-done
  946.3 0.0 slice-done.1
  946.3 0.0 slice-done.2
  946.3 0.0 slice-done.3
  946.3 6.2 copy.63
  (24 shorter events, 0.3 us)
Async XLA Ops:
  7.2 646.8 %all-gather.6.cloned.1.call-start = ((), (), s32[]{:S(2)}) async-start(), calls=%async_computation.6 | async-start | bytes 20971520 | tf_op jit(solution)/shard_map/all_gather | solution.py:24
  15.9 8.7 copy-start.3
  309.3 360.9 %all-gather.8.cloned.1.call-start = ((), (), s32[]{:S(2)}) async-start(), calls=%async_computation.7 | async-start | bytes 20971520 | tf_op jit(solution)/shard_map/all_gather | solution.py:26
  315.4 420.5 %all-gather.4.cloned.1.call-start = ((), (), s32[]{:S(2)}) async-start(), calls=%async_computation.5 | async-start | bytes 20971520 | tf_op jit(solution)/shard_map/all_gather | solution.py:23
  625.2 6.7 copy-start.1
  625.2 16.2 %copy-start = (bf16[768,2048]{1,0:T(8,128)(2,1)S(1)}, bf16[768,2048]{1,0:T(8,128)(2,1)}, u32[]{:S(2)}) copy-start(bf16[768,2048]{1,0:T(8,128)(2,1)} %param.9) | copy-start | bytes 9437188
  631.8 282.1 %reduce-scatter.2.cloned.1.call-start = ((), (), s32[]{:S(2)}) async-start(), calls=%async_computation.8 | async-start | bytes 7077888 | tf_op jit(solution)/shard_map/reduce_scatter | solution.py:60
  644.9 8.9 copy-start.2
  915.8 30.5 %slice-start = ((s8[16777216]{0:T(1024)(128)(4,1)}), s8[4194304]{0:T(1024)(128)(4,1)S(1)}, s32[]{:S(2)}) async-start(s8[16777216]{0:T(1024)(128)(4,1)} %bitcast.53), calls=%async_computation.9 | async-start | bytes 8388608
  915.8 30.5 %slice-start.1 = ((s8[16777216]{0:T(1024)(128)(4,1)}), s8[4194304]{0:T(1024)(128)(4,1)S(1)}, s32[]{:S(2)}) async-start(s8[16777216]{0:T(1024)(128)(4,1)} %bitcast.53), calls=%async_computation.10 | async-start | bytes 8388608
  931.1 15.2 %slice-start.2 = ((s8[16777216]{0:T(1024)(128)(4,1)}), s8[4194304]{0:T(1024)(128)(4,1)S(1)}, s32[]{:S(2)}) async-start(s8[16777216]{0:T(1024)(128)(4,1)} %bitcast.53), calls=%async_computation.11 | async-start | bytes 8388608
  931.1 15.2 %slice-start.3 = ((s8[16777216]{0:T(1024)(128)(4,1)}), s8[4194304]{0:T(1024)(128)(4,1)S(1)}, s32[]{:S(2)}) async-start(s8[16777216]{0:T(1024)(128)(4,1)} %bitcast.53), calls=%async_computation.12 | async-start | bytes 8388608
Sparse Core Ops, SparseCore 0:
  309.4 148.9 all-gather.5
  460.0 104.8 all-gather.7
  631.9 103.9 all-gather.3
  795.8 118.0 reduce-scatter.1
where the time goes:
time: 961 us; the launch traced here: 959 us
  blocking collectives  347 us (36%)
  local copies, waits for them, and re-layouts  252 us (26%)
  waiting for transfers between devices  184 us (19%)
  other arithmetic  118 us (12%)
  matrix products  43.5 us (5%)
  between operations  14 us (1%)
    reduce_scatter x1, waiting for transfers between devices, shards(): lax.psum_scatter(shares[:, 0:1] * first_rows + shares[:, 1:2] * second_ro...  118 us
    all_to_all x1, blocking collectives, shards(): lax.all_to_all(up_one, 'fs', split_axis=2, concat_axis=1, tiled=True)  99.8 us
    unnamed x28, local copies, waits for them, and re-layouts  98.2 us
    all_to_all x1, blocking collectives, shards(): lax.all_to_all(gate_one, 'fs', split_axis=2, concat_axis=1, tiled=True)  97.7 us
    all_to_all x1, blocking collectives, shards(): lax.all_to_all(gate_part, 'tp', split_axis=0, concat_axis=2, tiled=True)  97.4 us
    unnamed x4, other arithmetic  87.2 us
    all_gather x1, waiting for transfers between devices, shards(): lax.all_gather(gate_mine, 'tp', axis=0, tiled=True)  65.7 us
    all_to_all x1, blocking collectives, shards(): lax.all_to_all(up_part, 'tp', split_axis=0, concat_axis=2, tiled=True)  52.6 us
  transfers between devices with their start and end apart: 4, of which 2 were waited for; matrix products, arithmetic and copies ran while one was open for 17% of the time, Pallas kernels for 0%

commit v1 on v0

--- a/solution.py
+++ b/solution.py
@@ -4,6 +4,26 @@
 from jax.sharding import PartitionSpec as P
 
 EPS = 0.5
+
+
+def see_pages(field_in, bus_axis):
+    item_now, u_next = (lax.psum(1, axis_name=bus_axis), lax.axis_index(bus_axis))
+    then = field_in.shape[2] // item_now
+    state_now = jnp.roll(field_in, -u_next * then, 2)
+    line_up = [lax.slice_in_dim(state_now, 0, then, axis=2)]
+    num = 1
+    while num < item_now:
+        small = lax.slice_in_dim(state_now, num * then, (num + 1) * then, axis=2)
+        line_up.append(
+            lax.ppermute(
+                small,
+                axis_name=bus_axis,
+                perm=[(tick, (tick + num) % item_now) for tick in range(item_now)],
+            )
+        )
+        num = num + 1
+    q_next = jnp.roll(jnp.concatenate(line_up[::-1], 1), (u_next + 1) * line_up[0].shape[1], 1)
+    return q_next
 
 
 def shards(tokens, norm_gain, gate_weight, up_weight, down_weight, routes, route_logit):
@@ -16,7 +36,7 @@
         lax.all_to_all(up_part, "tp", split_axis=0, concat_axis=2, tiled=True),
     )
     gate_mine, up_mine = (
-        lax.all_to_all(gate_one, "fs", split_axis=2, concat_axis=1, tiled=True),
+        see_pages(gate_one, "fs"),
         lax.all_to_all(up_one, "fs", split_axis=2, concat_axis=1, tiled=True),
     )
     gate_out, up_out = (

time: 961 us -> 898 us (0.934)
  waiting for transfers between devices: 184 us -> 407 us
  blocking collectives: 347 us -> 152 us
  local copies, waits for them, and re-layouts: 252 us -> 189 us
  other arithmetic: 118 us -> 77.4 us
  starting transfers between devices: 0.16 us -> 13.2 us
    all_to_all x2 -> x0, blocking collectives: 195 us -> none  [the longest x1 97.7 us: shards(): lax.all_to_all(gate_one, 'fs', split_axis=2, concat_axis=1, tiled=True)]
    all_to_all x0 -> x1, waiting for transfers between devices: none -> 93.3 us  [shards(): lax.all_to_all(gate_part, 'tp', split_axis=0, concat_axis=2, tiled=True)]
    ppermute x0 -> x7, waiting for transfers between devices: none -> 85.6 us  [see_pages(): lax.ppermute(small, axis_name=bus_axis, perm=[(tick, (tick + num) % item_...]
    unnamed x4 -> x3, other arithmetic: 87.2 us -> 43.6 us
    all_to_all x1, local copies, waits for them, and re-layouts: 49.3 us -> 6.32 us  [shards(): lax.all_to_all(gate_part, 'tp', split_axis=0, concat_axis=2, tiled=True)]
    all_gather x1, waiting for transfers between devices: 65.7 us -> 108 us  [shards(): lax.all_gather(gate_mine, 'tp', axis=0, tiled=True)]
    unnamed x28 -> x42, local copies, waits for them, and re-layouts: 98.2 us -> 79.9 us
  transfers between devices with their start and end apart: 4 -> 12, of which waited for: 2 -> 9; matrix products, arithmetic and copies ran while one was open for 17% -> 7% of each run, Pallas kernels for 0% -> 0%
where the time goes in v1:
time: 898 us; the launch traced here: 897 us
  waiting for transfers between devices  407 us (45%)
  local copies, waits for them, and re-layouts  189 us (21%)
  blocking collectives  152 us (17%)
  other arithmetic  77.4 us (9%)
  matrix products  43.4 us (5%)
  between operations  14.1 us (2%)
  starting transfers between devices  13.2 us (1%)
    reduce_scatter x1, waiting for transfers between devices, shards(): lax.psum_scatter(shares[:, 0:1] * first_rows + shares[:, 1:2] * second_ro...  118 us
    all_gather x1, waiting for transfers between devices, shards(): lax.all_gather(gate_mine, 'tp', axis=0, tiled=True)  108 us
    all_to_all x1, blocking collectives, shards(): lax.all_to_all(up_one, 'fs', split_axis=2, concat_axis=1, tiled=True)  99.8 us
    all_to_all x1, waiting for transfers between devices, shards(): lax.all_to_all(gate_part, 'tp', split_axis=0, concat_axis=2, tiled=True)  93.3 us
    ppermute x7, waiting for transfers between devices, see_pages(): lax.ppermute(small, axis_name=bus_axis, perm=[(tick, (tick + num) % item_...  85.6 us
    unnamed x42, local copies, waits for them, and re-layouts  79.9 us
    all_to_all x1, blocking collectives, shards(): lax.all_to_all(up_part, 'tp', split_axis=0, concat_axis=2, tiled=True)  52.6 us
    all_to_all x1, local copies, waits for them, and re-layouts, shards(): lax.all_to_all(up_part, 'tp', split_axis=0, concat_axis=2, tiled=True)  49.3 us
  transfers between devices with their start and end apart: 12, of which 9 were waited for; matrix products, arithmetic and copies ran while one was open for 7% of the time, Pallas kernels for 0%

profile of v1, /device:TPU:0, one launch (start us, length us, event | category | flops | bytes accessed | tf_op | source)
XLA Modules:
  0.0 897.0 jit_solution(12534869999038379009)
XLA Ops:
  7.2 0.0 all-gather.6.cloned.1.call-start
  7.2 8.7 copy.36
  15.9 8.7 copy.39
  24.6 10.7 %multiply_convert_fusion = (bf16[4,256,2048]{1,2,0:T(8,128)(2,1)}, bf16[4,256,2048]{1,2,0:T(8,128)(2,1)}) fusion(f32[4,256,2048]{1,2,0:T(8,128)} %copy.39, f32[256]{0:T(256)S(1)} %copy-done.4, f32[4,256,2048]{1,2,0:T(8,128)} %copy.36), kind=kLoop, calls=%fused_computation.6 | loop fusion | flops 8388608 | bytes 25166848 | tf_op jit(solution)/shard_map/convert_element_type | solution.py:32
  35.3 52.6 %all_to_all.54 = bf16[4,256,2048]{1,2,0:T(8,128)(2,1)S(1)} all-to-all(bf16[4,256,2048]{1,2,0:T(8,128)(2,1)} %get-tuple-element.16), channel_id=1, replica_groups=mesh['fs'=8,'tp'=4] {'tp'}, dimensions={0} | all-to-all | bytes 8388608 | tf_op jit(solution)/shard_map/all_to_all | solution.py:36
  87.9 49.3 %copy.47 = bf16[1,256,8192]{1,0,2:T(2,128)(2,1)} copy(bf16[1,256,8192]{1,2,0:T(8,128)(2,1)S(1)} %bitcast.39) | data formatting | bytes 8388608 | tf_op jit(solution)/shard_map/all_to_all | solution.py:36
  137.2 0.5 broadcast.80
  137.7 43.5 %reduce.12 = bf16[8192,256]{1,0:T(8,128)(2,1)} reduce(bf16[8192,1,256]{2,1,0:T(2,128)(2,1)} %bitcast.37, bf16[]{:T(256)} %broadcast.80), dimensions={1}, to_apply=%bitcast.33.reduce_sub_computation | reduce | bytes 8388610
  181.2 6.9 reshape.135
  188.2 99.8 %all_to_all.55 = bf16[8,2,131072]{2,1,0:T(2,128)(2,1)} all-to-all(bf16[8,2,131072]{2,1,0:T(2,128)(2,1)} %reshape.135), channel_id=1, replica_groups=mesh['fs'=8,'tp'=4] {'fs'}, dimensions={0} | all-to-all | bytes 8388608 | tf_op jit(solution)/shard_map/all_to_all | solution.py:40
  288.0 8.7 reshape.136
  296.7 6.1 copy.43
  302.8 6.4 copy.41
  309.3 0.0 all-gather.6.cloned.1.call-update
  309.3 0.0 all-gather.8.cloned.1.call-start
  309.3 6.0 convert_element_type.26
  315.4 5.0 all-to-all-start
  320.4 0.2 all-gather.4.cloned.1.call-start
  320.7 93.3 %all-to-all-done = bf16[4,256,2048]{1,2,0:T(8,128)(2,1)} async-done(((bf16[4,256,2048]{1,2,0:T(8,128)(2,1)}), bf16[4,256,2048]{1,2,0:T(8,128)(2,1)}, u32[]{:S(2)}, u32[]{:S(2)}) %all-to-all-start) | async-done | bytes 4194336 | tf_op jit(solution)/shard_map/all_to_all | solution.py:35
  414.0 6.3 copy.37
  420.3 3.2 fusion.5
  423.5 2.0 copy-done
  425.5 1.7 fusion.18
  427.3 1.7 collective-permute-start
  429.0 2.0 collective-permute-start.2
  430.9 1.0 collective-permute-start.3
  432.0 2.3 collective-permute-start.4
  434.3 7.4 collective-permute-done
  441.7 0.8 collective-permute-start.5
  442.6 10.4 %collective-permute-done.1 = bf16[1,256,1024]{2,1,0:T(8,128)(2,1)S(1)} collective-permute-done((bf16[1,256,1024]{2,1,0:T(8,128)(2,1)}, bf16[1,256,1024]{2,1,0:T(8,128)(2,1)S(1)}, u32[]{:S(2)}, u32[]{:S(2)}) %collective-permute-start.1) | collective-permute-done | bytes 524320 | tf_op jit(solution)/shard_map/ppermute | solution.py:18
  453.0 11.2 %collective-permute-done.2 = bf16[1,256,1024]{2,1,0:T(8,128)(2,1)S(1)} collective-permute-done((bf16[1,256,1024]{2,1,0:T(8,128)(2,1)}, bf16[1,256,1024]{2,1,0:T(8,128)(2,1)S(1)}, u32[]{:S(2)}, u32[]{:S(2)}) %collective-permute-start.2) | collective-permute-done | bytes 524320 | tf_op jit(solution)/shard_map/ppermute | solution.py:18
  464.2 54.9 %collective-permute-done.3 = bf16[1,256,1024]{2,1,0:T(8,128)(2,1)S(1)} collective-permute-done((bf16[1,256,1024]{2,1,0:T(8,128)(2,1)}, bf16[1,256,1024]{2,1,0:T(8,128)(2,1)S(1)}, u32[]{:S(2)}, u32[]{:S(2)}) %collective-permute-start.3) | collective-permute-done | bytes 524320 | tf_op jit(solution)/shard_map/ppermute | solution.py:18
  519.2 1.7 collective-permute-done.4
  521.0 1.1 slice_dynamic-update-slice_fusion
  522.4 1.2 slice_dynamic-update-slice_fusion.1
  523.7 2.5 constant_dynamic-slice_fusion
  526.1 0.0 all-gather.4.cloned.1.call-update
  526.2 0.0 reduce-scatter.2.cloned.1.call-start
  526.3 1.1 reduce-window.6
  527.4 0.2 slice_reduce_fusion
  527.6 0.2 reduce-window.9
  527.8 0.1 add_bitcast_fusion
  527.9 0.2 copy.42
  528.1 0.3 reshape.85
  528.4 0.8 reshape.116
  529.3 6.3 scatter_custom_fusion
  535.7 0.1 broadcast_in_dim.37
  535.8 0.7 fusion.2
  536.5 2.5 fusion.3
  538.9 8.6 gather_fusion
  547.7 0.0 all-gather.6.cloned.1.call-done
  547.7 16.2 %fusion = f32[4,480,1024]{2,1,0:T(8,128)} fusion(bf16[4,2048,1024]{2,1,0:T(8,128)(2,1)} %all-gather.6.cloned.1.call-done, bf16[4,480,2048]{2,1,0:T(8,128)(2,1)} %bitcast.44, pred[4,480]{1,0:T(4,128)(4,1)S(1)} %broadcast_in_dim.37), kind=kOutput, calls=%fused_computation.12 | convolution fusion | flops 8056995840 | bytes 32507776 | tf_op jit(solution)/shard_map/ecd,edf->ecf/dot_general | solution.py:74
  563.9 1.9 all-gather.8.cloned.1.call-done
  565.8 108.1 %all-gather.4.cloned.1.call-done = bf16[4,2048,1024]{2,1,0:T(8,128)(2,1)} async-done(((bf16[1,2048,1024]{2,1,0:T(8,128)(2,1)}), bf16[4,2048,1024]{2,1,0:T(8,128)(2,1)}) %all-gather.4.cloned.1.call-update) | async-done | bytes 16777232 | tf_op jit(solution)/shard_map/all_gather | solution.py:43
  673.9 27.2 %fusion.8 = f32[4,480,2048]{2,1,0:T(8,128)} fusion(bf16[4,1024,2048]{2,1,0:T(8,128)(2,1)} %all-gather.8.cloned.1.call-done, f32[4,480,1024]{2,1,0:T(8,128)} %fusion, bf16[4,2048,1024]{2,1,0:T(8,128)(2,1)} %all-gather.4.cloned.1.call-done, bf16[4,480,2048]{2,1,0:T(8,128)(2,1)} %bitcast.45, pred[4,480]{1,0:T(4,128)(4,1)S(1)} %broadcast_in_dim.37), kind=kOutput, calls=%fused_computation.22 | convolution fusion | flops 16121856000 | bytes 65013632 | tf_op jit(solution)/shard_map/ecf,efd->ecd/dot_general | solution.py:76
  701.1 12.7 %gather_fusion.1 = f32[768,2048]{1,0:T(8,128)} fusion(f32[1920,2048]{1,0:T(8,128)} %bitcast.35, s32[1024]{0:T(1024)S(1)} %get-tuple-element.19), kind=kCustom, calls=%fused_computation.clone | custom fusion | bytes 12585984 | tf_op jit(solution)/shard_map/jit(_take)/gather | solution.py:78
  713.8 12.7 %gather_fusion.2 = f32[768,2048]{1,0:T(8,128)} fusion(f32[1920,2048]{1,0:T(8,128)} %bitcast.36, s32[1024]{0:T(1024)S(1)} %get-tuple-element.18), kind=kCustom, calls=%fused_computation.1.clone | custom fusion | bytes 12585984 | tf_op jit(solution)/shard_map/jit(_take)/gather | solution.py:79
  726.4 7.2 fusion.4
  733.7 0.0 reduce-scatter.2.cloned.1.call-update
  733.7 118.2 %reduce-scatter.2.cloned.1.call-done = f32[96,2048]{1,0:T(8,128)} async-done(((f32[768,2048]{1,0:T(8,128)}), f32[96,2048]{1,0:T(8,128)}) %reduce-scatter.2.cloned.1.call-update) | async-done | bytes 786448 | tf_op jit(solution)/shard_map/reduce_scatter | solution.py:80
  851.8 1.9 convert_element_type.31
  853.8 15.2 %copy.66 = bf16[4,2048,1024]{2,1,0:T(8,128)(2,1)} copy(bf16[4,2048,1024]{2,1,0:T(8,128)(2,1)} %all-gather.4.cloned.1.call-done) | data formatting | bytes 33554432
  869.0 15.2 %copy.67 = bf16[4,2048,1024]{2,1,0:T(8,128)(2,1)} copy(bf16[4,2048,1024]{2,1,0:T(8,128)(2,1)} %all-gather.6.cloned.1.call-done) | data formatting | bytes 33554432
  884.3 6.2 copy.68
  (54 shorter events, 0.8 us)
Async XLA Ops:
  7.2 540.6 %all-gather.6.cloned.1.call-start = ((), (), s32[]{:S(2)}) async-start(), calls=%async_computation.5 | async-start | bytes 20971520 | tf_op jit(solution)/shard_map/all_gather | solution.py:44
  15.9 8.7 copy-start.4
  309.3 256.5 %all-gather.8.cloned.1.call-start = ((), (), s32[]{:S(2)}) async-start(), calls=%async_computation.6 | async-start | bytes 20971520 | tf_op jit(solution)/shard_map/all_gather | solution.py:46
  315.4 98.6 %all-to-all-start = ((bf16[4,256,2048]{1,2,0:T(8,128)(2,1)}), bf16[4,256,2048]{1,2,0:T(8,128)(2,1)}, u32[]{:S(2)}, u32[]{:S(2)}) async-start(bf16[4,256,2048]{1,2,0:T(8,128)(2,1)} %get-tuple-element.17), calls=%async_computation | async-start | bytes 8388608 | tf_op jit(solution)/shard_map/all_to_all | solution.py:35
  320.4 353.4 %all-gather.4.cloned.1.call-start = ((), (), s32[]{:S(2)}) async-start(), calls=%async_computation.4 | async-start | bytes 20971520 | tf_op jit(solution)/shard_map/all_gather | solution.py:43
  423.5 2.0 copy-start
  427.3 14.4 %collective-permute-start = (bf16[1,256,1024]{2,1,0:T(8,128)(2,1)}, bf16[1,256,1024]{2,1,0:T(8,128)(2,1)S(1)}, u32[]{:S(2)}, u32[]{:S(2)}) collective-permute-start(bf16[1,256,1024]{2,1,0:T(8,128)(2,1)} %get-tuple-element.15), channel_id=1, source_target_pairs={{0,28},{4,0},{8,4},{12,8},{16,12},{20,16},{24,20},{28,24},{1,29},{... | collective-permute-start | bytes 1572872 | tf_op jit(solution)/shard_map/ppermute | solution.py:18
  429.0 23.9 %collective-permute-start.1 = (bf16[1,256,1024]{2,1,0:T(8,128)(2,1)}, bf16[1,256,1024]{2,1,0:T(8,128)(2,1)S(1)}, u32[]{:S(2)}, u32[]{:S(2)}) collective-permute-start(bf16[1,256,1024]{2,1,0:T(8,128)(2,1)} %get-tuple-element.14), channel_id=1, source_target_pairs={{0,24},{4,28},{8,0},{12,4},{16,8},{20,12},{24,16},{28,20},{1,25},{... | collective-permute-start | bytes 1572872 | tf_op jit(solution)/shard_map/ppermute | solution.py:18
  429.0 35.2 %collective-permute-start.2 = (bf16[1,256,1024]{2,1,0:T(8,128)(2,1)}, bf16[1,256,1024]{2,1,0:T(8,128)(2,1)S(1)}, u32[]{:S(2)}, u32[]{:S(2)}) collective-permute-start(bf16[1,256,1024]{2,1,0:T(8,128)(2,1)} %get-tuple-element.13), channel_id=1, source_target_pairs={{0,20},{4,24},{8,28},{12,0},{16,4},{20,8},{24,12},{28,16},{1,21},{... | collective-permute-start | bytes 1572872 | tf_op jit(solution)/shard_map/ppermute | solution.py:18
  430.9 88.2 %collective-permute-start.3 = (bf16[1,256,1024]{2,1,0:T(8,128)(2,1)}, bf16[1,256,1024]{2,1,0:T(8,128)(2,1)S(1)}, u32[]{:S(2)}, u32[]{:S(2)}) collective-permute-start(bf16[1,256,1024]{2,1,0:T(8,128)(2,1)} %get-tuple-element.12), channel_id=1, source_target_pairs={{0,16},{4,20},{8,24},{12,28},{16,0},{20,4},{24,8},{28,12},{1,17},{... | collective-permute-start | bytes 1572872 | tf_op jit(solution)/shard_map/ppermute | solution.py:18
  432.0 88.9 %collective-permute-start.4 = (bf16[1,256,1024]{2,1,0:T(8,128)(2,1)}, bf16[1,256,1024]{2,1,0:T(8,128)(2,1)S(1)}, u32[]{:S(2)}, u32[]{:S(2)}) collective-permute-start(bf16[1,256,1024]{2,1,0:T(8,128)(2,1)} %get-tuple-element.11), channel_id=1, source_target_pairs={{0,12},{4,16},{8,20},{12,24},{16,28},{20,0},{24,4},{28,8},{1,13},{... | collective-permute-start | bytes 1572872 | tf_op jit(solution)/shard_map/ppermute | solution.py:18
  441.7 79.2 %collective-permute-start.5 = (bf16[1,256,1024]{2,1,0:T(8,128)(2,1)}, bf16[1,256,1024]{2,1,0:T(8,128)(2,1)S(1)}, u32[]{:S(2)}, u32[]{:S(2)}) collective-permute-start(bf16[1,256,1024]{2,1,0:T(8,128)(2,1)} %get-tuple-element.10), channel_id=1, source_target_pairs={{0,8},{4,12},{8,16},{12,20},{16,24},{20,28},{24,0},{28,4},{1,9},{5... | collective-permute-start | bytes 1572872 | tf_op jit(solution)/shard_map/ppermute | solution.py:18
  452.9 68.1 %collective-permute-start.6 = (bf16[1,256,1024]{2,1,0:T(8,128)(2,1)S(1)}, bf16[1,256,1024]{2,1,0:T(8,128)(2,1)S(1)}, u32[]{:S(2)}, u32[]{:S(2)}) collective-permute-start(bf16[1,256,1024]{2,1,0:T(8,128)(2,1)S(1)} %get-tuple-element.9), channel_id=1, source_target_pairs={{0,4},{4,8},{8,12},{12,16},{16,20},{20,24},{24,28},{28,0},{1,5},{5... | collective-permute-start | bytes 1572872 | tf_op jit(solution)/shard_map/ppermute | solution.py:18
  522.3 3.9 copy-start.2
  522.4 13.4 %copy-start.1 = (bf16[768,2048]{1,0:T(8,128)(2,1)S(1)}, bf16[768,2048]{1,0:T(8,128)(2,1)}, u32[]{:S(2)}) copy-start(bf16[768,2048]{1,0:T(8,128)(2,1)} %param.9) | copy-start | bytes 9437188
  526.2 325.7 %reduce-scatter.2.cloned.1.call-start = ((), (), s32[]{:S(2)}) async-start(), calls=%async_computation.7 | async-start | bytes 7077888 | tf_op jit(solution)/shard_map/reduce_scatter | solution.py:80
  538.9 8.7 copy-start.3
  853.8 30.5 %slice-start = ((s8[16777216]{0:T(1024)(128)(4,1)}), s8[4194304]{0:T(1024)(128)(4,1)S(1)}, s32[]{:S(2)}) async-start(s8[16777216]{0:T(1024)(128)(4,1)} %bitcast.41), calls=%async_computation.8 | async-start | bytes 8388608
  853.8 30.5 %slice-start.1 = ((s8[16777216]{0:T(1024)(128)(4,1)}), s8[4194304]{0:T(1024)(128)(4,1)S(1)}, s32[]{:S(2)}) async-start(s8[16777216]{0:T(1024)(128)(4,1)} %bitcast.41), calls=%async_computation.9 | async-start | bytes 8388608
  869.0 15.2 %slice-start.2 = ((s8[16777216]{0:T(1024)(128)(4,1)}), s8[4194304]{0:T(1024)(128)(4,1)S(1)}, s32[]{:S(2)}) async-start(s8[16777216]{0:T(1024)(128)(4,1)} %bitcast.41), calls=%async_computation.10 | async-start | bytes 8388608
  869.0 15.2 %slice-start.3 = ((s8[16777216]{0:T(1024)(128)(4,1)}), s8[4194304]{0:T(1024)(128)(4,1)S(1)}, s32[]{:S(2)}) async-start(s8[16777216]{0:T(1024)(128)(4,1)} %bitcast.41), calls=%async_computation.11 | async-start | bytes 8388608
Sparse Core Ops, SparseCore 0:
  309.4 148.9 all-gather.5
  460.0 105.7 all-gather.7
  567.9 105.8 all-gather.3
  733.8 118.0 reduce-scatter.1
